TPU v7x, 32 devices: a whole 2x2x4 slice. The times are simulated.
32 devices in a mesh: kv: 4 (over y, x), tp: 8 (over z, core).
Axes of the slice: x: 2, y: 2, z: 4, core: 2. Of those that a mesh axis runs over, the one named last changes fastest.
Arguments:
- tokens: bfloat16 [64, 4096], P(None, ('kv', 'tp')), may hold values from -6 to 6
- memory: float32 [64, 16, 256, 128], P('kv', 'tp'), may hold values from -6 to 6
- normalizer: float32 [64, 16, 128], P('kv', 'tp'), may hold values from -6 to 6
- stabilizer: float32 [64, 16], P('kv', 'tp'), may hold values from -4 to 4
- first_gain: float32 [4096], replicated, may hold values from 0.1 to 1.9
- first_gate: bfloat16 [4096, 12288], P('kv', 'tp'), may hold values from -0.09375 to 0.09375
- first_up: bfloat16 [4096, 12288], P('kv', 'tp'), may hold values from -0.09375 to 0.09375
- first_down: bfloat16 [12288, 4096], P('tp', 'kv'), may hold values from -0.078125 to 0.078125
- mixer_gain: float32 [4096], replicated, may hold values from 0.1 to 1.9
- query_weight: bfloat16 [4096, 2048], P(None, 'tp'), may hold values from -0.09375 to 0.09375
- key_weight: bfloat16 [4096, 2048], P(None, 'tp'), may hold values from -0.09375 to 0.09375
- value_weight: bfloat16 [4096, 4096], P(None, 'tp'), may hold values from -0.09375 to 0.09375
- input_weight: bfloat16 [4096, 16], replicated, may hold values from -0.09375 to 0.09375
- forget_weight: bfloat16 [4096, 16], replicated, may hold values from -0.09375 to 0.09375
- forget_bias: float32 [16], P('tp'), may hold values from -2 to 4
- output_weight: bfloat16 [4096, 4096], P('tp'), may hold values from -0.09375 to 0.09375
- last_gain: float32 [4096], replicated, may hold values from 0.1 to 1.9
- last_gate: bfloat16 [4096, 12288], P('kv', 'tp'), may hold values from -0.09375 to 0.09375
- last_up: bfloat16 [4096, 12288], P('kv', 'tp'), may hold values from -0.09375 to 0.09375
- last_down: bfloat16 [12288, 4096], P('tp', 'kv'), may hold values from -0.078125 to 0.078125
Outputs:
- result: bfloat16 [64, 4096], P(None, ('kv', 'tp'))
- new_memory: float32 [64, 16, 256, 128], P('kv', 'tp')
- new_normalizer: float32 [64, 16, 128], P('kv', 'tp')
- new_stabilizer: float32 [64, 16], P('kv', 'tp')
All inputs are finite; a program needn't handle non-finite values.
Results may differ from a plain program's by a relative error of at most 0.025.
Values may be sent and summed in bfloat16 or wider, within the bound.
A program may use at most 128 MiB of HBM per device.

v0:
```python
import jax
import jax.numpy as jnp
from jax import lax
from jax.sharding import PartitionSpec as P

EPS = 1e-06


def hidden_units(gate_acc, up_acc, squares, model_width):
    scale = lax.rsqrt(squares / model_width + EPS)[:, None]
    return (jax.nn.silu(scale * gate_acc) * (scale * up_acc)).astype(jnp.bfloat16)


def gated_block(block, gain, w_gate, w_up, w_down, model_width):
    f32 = jnp.float32
    width = block.shape[1]
    gain_block = lax.dynamic_slice_in_dim(gain, lax.axis_index("kv") * width, width, 0)
    values = block.astype(f32)
    scaled = (values * gain_block).astype(jnp.bfloat16)
    gate_part = jnp.dot(scaled, w_gate, preferred_element_type=f32)
    up_part = jnp.dot(scaled, w_up, preferred_element_type=f32)
    squares = jnp.sum(values * values, axis=1)
    gate_acc, up_acc, sq_total = (
        lax.psum(gate_part.astype(jnp.bfloat16), "kv").astype(jnp.float32),
        lax.psum(up_part.astype(jnp.bfloat16), "kv").astype(jnp.float32),
        lax.psum(squares.astype(jnp.bfloat16), "kv").astype(jnp.float32),
    )
    hidden = hidden_units(gate_acc, up_acc, sq_total, model_width)
    share = lax.psum_scatter(
        lax.dot_general(
            w_down, hidden, (((0,), (1,)), ((), ())), preferred_element_type=f32
        ).astype(jnp.bfloat16),
        "tp",
        scatter_dimension=0,
        tiled=True,
    ).astype(jnp.float32)
    return share.T


def body(
    tokens,
    memory,
    normalizer,
    stabilizer,
    first_gain,
    first_gate,
    first_up,
    first_down,
    mixer_gain,
    query_weight,
    key_weight,
    value_weight,
    input_weight,
    forget_weight,
    forget_bias,
    output_weight,
    last_gain,
    last_gate,
    last_up,
    last_down,
):
    f32 = jnp.float32
    model_width = first_gain.shape[0]
    rows, col_width = tokens.shape
    block = lax.all_gather(tokens, "tp", axis=1, tiled=True)
    first_share = gated_block(block, first_gain, first_gate, first_up, first_down, model_width)
    stream_one = (tokens.astype(f32) + 0.5 * first_share).astype(jnp.bfloat16)
    seq_count, head_count, value_size, key_size = memory.shape
    moved = lax.all_to_all(
        stream_one.reshape(rows, 1, col_width), "kv", split_axis=0, concat_axis=1, tiled=True
    )
    own_rows = lax.all_gather(moved, "tp", axis=2, tiled=True).reshape(seq_count, model_width)
    row_values = own_rows.astype(f32)
    scale = lax.rsqrt(jnp.mean(row_values * row_values, axis=1, keepdims=True) + EPS)
    cell_in = (row_values * mixer_gain).astype(jnp.bfloat16)
    query = (
        scale * jnp.dot(cell_in, query_weight, preferred_element_type=f32) * key_size ** (-0.5)
    ).reshape(seq_count, head_count, key_size)
    key = (scale * jnp.dot(cell_in, key_weight, preferred_element_type=f32)).reshape(
        seq_count, head_count, key_size
    )
    value = (scale * jnp.dot(cell_in, value_weight, preferred_element_type=f32)).reshape(
        seq_count, head_count, value_size
    )
    first_head = lax.axis_index("tp") * head_count
    input_all = scale * jnp.dot(cell_in, input_weight, preferred_element_type=f32)
    forget_all = scale * jnp.dot(cell_in, forget_weight, preferred_element_type=f32)
    input_pre = lax.dynamic_slice_in_dim(input_all, first_head, head_count, 1)
    log_forget = jax.nn.log_sigmoid(
        lax.dynamic_slice_in_dim(forget_all, first_head, head_count, 1) + forget_bias
    )
    carried = log_forget + stabilizer
    new_stabilizer = jnp.maximum(carried, input_pre)
    keep = jnp.exp(carried - new_stabilizer)
    admit = jnp.exp(input_pre - new_stabilizer)
    recalled = jnp.einsum("bhvd,bhd->bhv", memory, query, precision=lax.Precision.HIGHEST)
    match = jnp.sum(query * key, axis=-1)
    numer = keep[..., None] * recalled + (admit * match)[..., None] * value
    denom = keep * jnp.sum(normalizer * query, axis=-1) + admit * match
    cell_out = (
        (numer / jnp.maximum(jnp.abs(denom), 1.0)[..., None])
        .reshape(seq_count, head_count * value_size)
        .astype(jnp.bfloat16)
    )
    new_memory = (
        keep[..., None, None] * memory
        + admit[..., None, None] * value[..., :, None] * key[..., None, :]
    )
    new_normalizer = keep[..., None] * normalizer + admit[..., None] * key
    partial_heads = jnp.dot(cell_out, output_weight, preferred_element_type=f32)
    mixed = lax.psum(partial_heads.astype(jnp.bfloat16), "tp").astype(jnp.float32)
    rows_two = (row_values + mixed).astype(jnp.bfloat16)
    whole_two = lax.all_to_all(rows_two, "kv", split_axis=1, concat_axis=0, tiled=True)
    last_share = gated_block(whole_two, last_gain, last_gate, last_up, last_down, model_width)
    own_columns = lax.dynamic_slice_in_dim(
        whole_two, lax.axis_index("tp") * col_width, col_width, 1
    )
    result = (own_columns.astype(f32) + 0.5 * last_share).astype(jnp.bfloat16)
    return (result, new_memory, new_normalizer, new_stabilizer)


def solution(mesh):
    in_specs = (
        P(None, ("kv", "tp")),
        P("kv", "tp", None, None),
        P("kv", "tp", None),
        P("kv", "tp"),
        P(),
        P("kv", "tp"),
        P("kv", "tp"),
        P("tp", "kv"),
        P(),
        P(None, "tp"),
        P(None, "tp"),
        P(None, "tp"),
        P(),
        P(),
        P("tp"),
        P("tp", None),
        P(),
        P("kv", "tp"),
        P("kv", "tp"),
        P("tp", "kv"),
    )
    out_specs = (
        P(None, ("kv", "tp")),
        P("kv", "tp", None, None),
        P("kv", "tp", None),
        P("kv", "tp"),
    )
    return jax.shard_map(body, mesh=mesh, in_specs=in_specs, out_specs=out_specs, check_vma=False)
```

profile of v0, /device:TPU:0, one launch (start us, length us, event | category | flops | bytes accessed | tf_op | source)
XLA Modules:
  0.0 307.5 jit_solution(12249599025583255382)
XLA Ops:
  7.2 14.9 %all_gather.6 = bf16[64,1024]{1,0:T(8,128)(2,1)S(1)} all-gather(bf16[64,128]{1,0:T(8,128)(2,1)} %param.20), channel_id=1, replica_groups=mesh['kv'=4,'tp'=8] {'tp'}, dimensions={1}, use_global_device_ids=true | all-gather | bytes 147456 | tf_op jit(solution)/shard_map/all_gather | solution.py:65
  23.0 1.3 convolution_convert_fusion.3
  24.3 1.3 convolution_convert_fusion.4
  25.8 10.0 %psum.49 = bf16[64]{0:T(256)(128)(2,1)S(1)} all-reduce(bf16[64]{0:T(256)(128)(2,1)S(1)} %fusion.3), channel_id=1, replica_groups=mesh['kv'=4,'tp'=8] {'kv'}, use_global_device_ids=true, to_apply=%region_1.0 | all-reduce | flops 64 | bytes 256 | tf_op jit(solution)/shard_map/psum | solution.py:26
  35.8 34.0 %all-reduce.10.cloned.1.call-done = (bf16[64,1536]{1,0:T(8,128)(2,1)}, bf16[64,1536]{1,0:T(8,128)(2,1)}) async-done(((bf16[64,1536]{1,0:T(8,128)(2,1)}, bf16[64,1536]{1,0:T(8,128)(2,1)}), (bf16[64,1536]{1,0:T(8,128)(2,1)}, bf16[64,1536]{1,0:T(8,128)(2,1)})) %all-reduce.10.cloned.1.call-update) | async-done | bytes 393232 | tf_op jit(solution)/shard_map/psum | solution.py:25
  69.8 2.8 fusion
  73.5 30.9 %reduce-scatter.7.cloned.1.call-done = bf16[128,64]{1,0:T(8,128)(2,1)} async-done(((bf16[1024,64]{1,0:T(8,128)(2,1)}), bf16[128,64]{1,0:T(8,128)(2,1)}) %reduce-scatter.7.cloned.1.call-update) | async-done | bytes 16400
  107.1 3.7 %all-to-all-start = ((bf16[4,2,1024]{2,1,0:T(2,128)(2,1)}), bf16[4,2,1024]{2,1,0:T(2,128)(2,1)S(1)}, u32[]{:S(2)}, u32[]{:S(2)}) async-start(bf16[4,2,1024]{2,1,0:T(2,128)(2,1)} %reshape.77), calls=%async_computation | async-start | bytes 32768 | tf_op jit(solution)/shard_map/all_to_all | solution.py:69
  110.8 4.7 %all-to-all-done = bf16[4,2,1024]{2,1,0:T(2,128)(2,1)S(1)} async-done(((bf16[4,2,1024]{2,1,0:T(2,128)(2,1)}), bf16[4,2,1024]{2,1,0:T(2,128)(2,1)S(1)}, u32[]{:S(2)}, u32[]{:S(2)}) %all-to-all-start) | async-done | bytes 16416 | tf_op jit(solution)/shard_map/all_to_all | solution.py:69
  115.5 12.8 %all-gather = bf16[16,4,1,1024]{3,0,1,2:T(8,128)(2,1)S(1)} all-gather(bf16[16,4,1,128]{3,0,1,2:T(8,128)(2,1)S(1)} %bitcast.73), channel_id=2, replica_groups=mesh['kv'=4,'tp'=8] {'tp'}, dimensions={3}, use_global_device_ids=true | all-gather | bytes 147456 | tf_op jit(solution)/shard_map/all_gather | solution.py:72
  129.4 1.9 fusion.2
  132.6 3.5 %convolution_multiply_fusion = f32[16,512]{1,0:T(8,128)} fusion(bf16[16,4096]{1,0:T(8,128)(2,1)S(1)} %multiply_convert_fusion.3, bf16[4096,512]{1,0:T(8,128)(2,1)} %param.31, f32[16]{0:T(128)} %copy-done.8), kind=kOutput, calls=%fused_computation.10 | convolution fusion | flops 67117056 | bytes 4358208 | tf_op jit(solution)/shard_map/dot_general | solution.py:82
  136.0 1.4 reshape.63
  137.4 2.6 convolution_multiply_fusion.1
  140.7 1.4 multiply_reduce_fusion.2
  142.2 1.3 copy.76
  143.5 1.3 copy.74
  144.8 1.1 fusion.26
  145.9 1.1 fusion.25
  147.0 1.4 abs_maximum_fusion
  148.7 5.8 %fusion.27 = f32[16,2,1,256]{3,2,1,0:T(1,128)S(1)} fusion(f32[16,2,128,1]{2,3,1,0:T(1,128)} %bitcast.71, f32[16,2,256,128]{3,2,1,0:T(8,128)} %param.21), kind=kOutput, calls=%fused_computation.61 | convolution fusion | flops 12582912 | bytes 4243456 | tf_op jit(solution)/shard_map/bhvd,bhd->bhv/dot_general | solution.py:96
  154.7 1.3 convolution_convert_fusion
  156.1 51.8 %all-reduce.6.cloned.1.call-done = bf16[16,4096]{1,0:T(8,128)(2,1)} async-done(((bf16[16,4096]{1,0:T(8,128)(2,1)}), bf16[16,4096]{1,0:T(8,128)(2,1)}) %all-reduce.6.cloned.1.call-update) | async-done | bytes 131088 | tf_op jit(solution)/shard_map/psum | solution.py:111
  209.5 3.6 %all-to-all-start.1 = ((bf16[16,4,1024]{2,0,1:T(8,128)(2,1)}), bf16[16,4,1024]{2,0,1:T(8,128)(2,1)S(1)}, u32[]{:S(2)}, u32[]{:S(2)}) async-start(bf16[16,4,1024]{2,0,1:T(8,128)(2,1)} %bitcast.63), calls=%async_computation.1 | async-start | bytes 262144 | tf_op jit(solution)/shard_map/all_to_all | solution.py:113
  213.8 4.3 %all-to-all-done.1 = bf16[16,4,1024]{2,0,1:T(8,128)(2,1)S(1)} async-done(((bf16[16,4,1024]{2,0,1:T(8,128)(2,1)}), bf16[16,4,1024]{2,0,1:T(8,128)(2,1)S(1)}, u32[]{:S(2)}, u32[]{:S(2)}) %all-to-all-start.1) | async-done | bytes 131104 | tf_op jit(solution)/shard_map/all_to_all | solution.py:113
  218.2 3.4 %convolution_convert_fusion.1 = bf16[64,1536]{1,0:T(8,128)(2,1)} fusion(bf16[1024,1536]{1,0:T(8,128)(2,1)} %param.38, bf16[64,1024]{1,0:T(8,128)(2,1)S(1)} %bitcast.66, f32[1024]{0:T(1024)S(1)} %dynamic_slice.19), kind=kOutput, calls=%fused_computation.2 | convolution fusion | flops 201621504 | bytes 3477504 | tf_op jit(solution)/shard_map/dot_general | solution.py:21
  221.5 1.3 convolution_convert_fusion.2
  223.1 8.5 %psum.53 = bf16[64]{0:T(256)(128)(2,1)S(1)} all-reduce(bf16[64]{0:T(256)(128)(2,1)S(1)} %convert_element_type.143), channel_id=1, replica_groups=mesh['kv'=4,'tp'=8] {'kv'}, use_global_device_ids=true, to_apply=%region_10.11 | all-reduce | flops 64 | bytes 256 | tf_op jit(solution)/shard_map/psum | solution.py:26
  231.6 33.2 %all-reduce.8.cloned.1.call-done = (bf16[64,1536]{1,0:T(8,128)(2,1)}, bf16[64,1536]{1,0:T(8,128)(2,1)}) async-done(((bf16[64,1536]{1,0:T(8,128)(2,1)}, bf16[64,1536]{1,0:T(8,128)(2,1)}), (bf16[64,1536]{1,0:T(8,128)(2,1)}, bf16[64,1536]{1,0:T(8,128)(2,1)})) %all-reduce.8.cloned.1.call-update) | async-done | bytes 393232 | tf_op jit(solution)/shard_map/psum | solution.py:25
  264.8 2.8 fusion.1
  268.5 4.2 %multiply_add_fusion = f32[16,2,256,128]{3,2,1,0:T(8,128)} fusion(f32[16,2,256,128]{3,2,1,0:T(8,128)} %param.21, f32[16,2,128]{2,1,0:T(2,128)S(1)} %reshape.62, f32[16,2,256]{2,1,0:T(2,128)S(1)} %get-tuple-element.15, f32[16,2]{1,0:T(8,128)S(1)} %copy.73), kind=kLoop, calls=%fused_computation.1 | loop fusion | flops 3145728 | bytes 8437888 | tf_op jit(solution)/shard_map/add | solution.py:106
  273.5 26.0 %reduce-scatter.9.cloned.1.call-done = bf16[128,64]{1,0:T(8,128)(2,1)} async-done(((bf16[1024,64]{1,0:T(8,128)(2,1)}), bf16[128,64]{1,0:T(8,128)(2,1)}) %reduce-scatter.9.cloned.1.call-update) | async-done | bytes 16400
  (65 shorter events, 13.7 us)
Async XLA Ops:
  7.2 15.8 %copy-start = (bf16[1024,1536]{1,0:T(8,128)(2,1)S(1)}, bf16[1024,1536]{1,0:T(8,128)(2,1)}, u32[]{:S(2)}) copy-start(bf16[1024,1536]{1,0:T(8,128)(2,1)} %param.26) | copy-start | bytes 9437188
  7.2 62.6 %all-reduce.10.cloned.1.call-start = ((), (), s32[]{:S(2)}) async-start(), calls=%async_computation.8 | async-start | bytes 786432 | tf_op jit(solution)/shard_map/psum | solution.py:25
  22.1 2.2 copy-start.2
  25.6 79.7 %copy-start.5 = (bf16[64,128]{1,0:T(8,128)(2,1)S(1)}, bf16[64,128]{1,0:T(8,128)(2,1)}, u32[]{:S(2)}) copy-start(bf16[64,128]{1,0:T(8,128)(2,1)} %param.20) | copy-start | bytes 49156
  25.6 78.8 %reduce-scatter.7.cloned.1.call-start = ((), (), s32[]{:S(2)}) async-start(), calls=%async_computation.5 | async-start | bytes 294912
  69.8 59.0 %copy-start.7 = (f32[4096]{0:T(1024)S(1)}, f32[4096]{0:T(1024)}, u32[]{:S(2)}) copy-start(f32[4096]{0:T(1024)} %param.28) | copy-start | bytes 49156
  107.1 8.4 %all-to-all-start = ((bf16[4,2,1024]{2,1,0:T(2,128)(2,1)}), bf16[4,2,1024]{2,1,0:T(2,128)(2,1)S(1)}, u32[]{:S(2)}, u32[]{:S(2)}) async-start(bf16[4,2,1024]{2,1,0:T(2,128)(2,1)} %reshape.77), calls=%async_computation | async-start | bytes 32768 | tf_op jit(solution)/shard_map/all_to_all | solution.py:69
  110.8 97.1 %all-reduce.6.cloned.1.call-start = ((), (), s32[]{:S(2)}) async-start(), calls=%async_computation.4 | async-start | bytes 262144 | tf_op jit(solution)/shard_map/psum | solution.py:111
  128.8 0.6 copy-start.8
  132.6 4.8 %copy-start.9 = (f32[16]{0:T(128)S(1)}, f32[16]{0:T(128)}, u32[]{:S(2)}) copy-start(f32[16]{0:T(128)} %copy-done.8) | copy-start | bytes 196
  147.0 7.6 %copy-start.4 = (f32[16,2,256]{2,1,0:T(2,128)S(1)}, f32[16,2,256]{2,1,0:T(2,128)}, u32[]{:S(2)}) copy-start(f32[16,2,256]{2,1,0:T(2,128)} %reshape.63) | copy-start | bytes 98308
  148.7 6.0 %copy-start.1 = (bf16[512,4096]{1,0:T(8,128)(2,1)S(1)}, bf16[512,4096]{1,0:T(8,128)(2,1)}, u32[]{:S(2)}) copy-start(bf16[512,4096]{1,0:T(8,128)(2,1)} %param.35) | copy-start | bytes 12582916
  209.5 8.7 %all-to-all-start.1 = ((bf16[16,4,1024]{2,0,1:T(8,128)(2,1)}), bf16[16,4,1024]{2,0,1:T(8,128)(2,1)S(1)}, u32[]{:S(2)}, u32[]{:S(2)}) async-start(bf16[16,4,1024]{2,0,1:T(8,128)(2,1)} %bitcast.63), calls=%async_computation.1 | async-start | bytes 262144 | tf_op jit(solution)/shard_map/all_to_all | solution.py:113
  213.1 51.7 %all-reduce.8.cloned.1.call-start = ((), (), s32[]{:S(2)}) async-start(), calls=%async_computation.7 | async-start | bytes 786432 | tf_op jit(solution)/shard_map/psum | solution.py:25
  218.2 3.4 %copy-start.3 = (bf16[1024,1536]{1,0:T(8,128)(2,1)S(1)}, bf16[1024,1536]{1,0:T(8,128)(2,1)}, u32[]{:S(2)}) copy-start(bf16[1024,1536]{1,0:T(8,128)(2,1)} %param.37) | copy-start | bytes 9437188
  222.9 76.6 %reduce-scatter.9.cloned.1.call-start = ((), (), s32[]{:S(2)}) async-start(), calls=%async_computation.6 | async-start | bytes 294912
  268.5 4.2 %copy-start.6 = (f32[16,2,128]{2,1,0:T(2,128)S(1)}, f32[16,2,128]{2,1,0:T(2,128)}, u32[]{:S(2)}) copy-start(f32[16,2,128]{2,1,0:T(2,128)} %param.22) | copy-start | bytes 49156
Sparse Core Ops, SparseCore 0:
  25.7 44.0 all-reduce.9
  73.6 30.7 reduce-scatter.6
  156.2 51.6 all-reduce.5
  223.0 41.7 all-reduce.7
  268.6 30.7 reduce-scatter.8
where the time goes:
time: 308 us; the launch traced here: 307 us
  waiting for transfers between devices  185 us (60%)
  blocking collectives  46.2 us (15%)
  matrix products  30.2 us (10%)
  local copies, waits for them, and re-layouts  14 us (5%)
  between operations  13.9 us (5%)
  other arithmetic  10.6 us (3%)
  starting transfers between devices  7.45 us (2%)
    psum x2, waiting for transfers between devices, gated_block(): lax.psum(up_part.astype(jnp.bfloat16), 'kv').astype(jnp.float32)  67.2 us
    unnamed x7, waiting for transfers between devices  57 us
    psum x1, waiting for transfers between devices, body(): lax.psum(partial_heads.astype(jnp.bfloat16), 'tp').astype(jnp.float32)  51.8 us
    psum x2, blocking collectives, gated_block(): lax.psum(squares.astype(jnp.bfloat16), 'kv').astype(jnp.float32)  18.5 us
    all_gather x1, blocking collectives, body(): block = lax.all_gather(tokens, 'tp', axis=1, tiled=True)  14.9 us
    all_gather x1, blocking collectives, body(): lax.all_gather(moved, 'tp', axis=2, tiled=True)  12.8 us
  transfers between devices with their start and end apart: 7, of which 7 were waited for; matrix products, arithmetic and copies ran while one was open for 2% of the time, Pallas kernels for 0%

commit v1 on v0

--- a/solution.py
+++ b/solution.py
@@ -4,6 +4,12 @@
 from jax.sharding import PartitionSpec as P
 
 EPS = 1e-06
+
+
+def gather_and_add(shard, axis):
+    blocks = lax.all_gather(shard, axis, axis=0, tiled=False)
+    total = blocks.sum(axis=0)
+    return total
 
 
 def hidden_units(gate_acc, up_acc, squares, model_width):
@@ -108,7 +114,7 @@
     )
     new_normalizer = keep[..., None] * normalizer + admit[..., None] * key
     partial_heads = jnp.dot(cell_out, output_weight, preferred_element_type=f32)
-    mixed = lax.psum(partial_heads.astype(jnp.bfloat16), "tp").astype(jnp.float32)
+    mixed = gather_and_add(partial_heads.astype(jnp.bfloat16), "tp").astype(jnp.float32)
     rows_two = (row_values + mixed).astype(jnp.bfloat16)
     whole_two = lax.all_to_all(rows_two, "kv", split_axis=1, concat_axis=0, tiled=True)
     last_share = gated_block(whole_two, last_gain, last_gate, last_up, last_down, model_width)

time: 308 us -> 267 us (0.87)
  waiting for transfers between devices: 185 us -> 153 us
  local copies, waits for them, and re-layouts: 14 us -> 7.1 us
    psum x1 -> x0, waiting for transfers between devices: 51.8 us -> none  [body(): lax.psum(partial_heads.astype(jnp.bfloat16), 'tp').astype(jnp.float32)]
    all_gather x0 -> x1, waiting for transfers between devices: none -> 19.1 us  [gather_and_add(): blocks = lax.all_gather(shard, axis, axis=0, tiled=False)]
where the time goes in v1:
time: 267 us; the launch traced here: 266 us
  waiting for transfers between devices  153 us (57%)
  blocking collectives  46.2 us (17%)
  matrix products  28.9 us (11%)
  between operations  14 us (5%)
  other arithmetic  9.67 us (4%)
  starting transfers between devices  7.45 us (3%)
  local copies, waits for them, and re-layouts  7.1 us (3%)
    psum x2, waiting for transfers between devices, gated_block(): lax.psum(up_part.astype(jnp.bfloat16), 'kv').astype(jnp.float32)  67.7 us
    unnamed x7, waiting for transfers between devices  57 us
    all_gather x1, waiting for transfers between devices, gather_and_add(): blocks = lax.all_gather(shard, axis, axis=0, tiled=False)  19.1 us
    psum x2, blocking collectives, gated_block(): lax.psum(squares.astype(jnp.bfloat16), 'kv').astype(jnp.float32)  18.5 us
    all_gather x1, blocking collectives, body(): block = lax.all_gather(tokens, 'tp', axis=1, tiled=True)  14.9 us
    all_gather x1, blocking collectives, body(): lax.all_gather(moved, 'tp', axis=2, tiled=True)  12.8 us
    dot_general x1, matrix products, body(): jnp.einsum('bhvd,bhd->bhv', memory, query, precision=lax.Precision.HIGHEST)  5.81 us
    dot_general x2, matrix products, gated_block(): lax.dot_general(w_down, hidden, (((0,), (1,)), ((), ())), preferred_eleme...  5.66 us
  transfers between devices with their start and end apart: 7, of which 7 were waited for; matrix products, arithmetic and copies ran while one was open for 2% of the time, Pallas kernels for 0%

profile of v1, /device:TPU:0, one launch (start us, length us, event | category | flops | bytes accessed | tf_op | source)
XLA Modules:
  0.0 266.2 jit_solution(9406851130459628984)
XLA Ops:
  7.2 14.9 %all_gather.12 = bf16[64,1024]{1,0:T(8,128)(2,1)S(1)} all-gather(bf16[64,128]{1,0:T(8,128)(2,1)} %param.20), channel_id=1, replica_groups=mesh['kv'=4,'tp'=8] {'tp'}, dimensions={1}, use_global_device_ids=true | all-gather | bytes 147456 | tf_op jit(solution)/shard_map/all_gather | solution.py:71
  22.1 0.8 dynamic_slice.15
  23.0 1.3 convolution_convert_fusion.3
  24.3 1.3 convolution_convert_fusion.4
  25.8 10.0 %psum.42 = bf16[64]{0:T(256)(128)(2,1)S(1)} all-reduce(bf16[64]{0:T(256)(128)(2,1)S(1)} %fusion.3), channel_id=1, replica_groups=mesh['kv'=4,'tp'=8] {'kv'}, use_global_device_ids=true, to_apply=%region_1.0 | all-reduce | flops 64 | bytes 256 | tf_op jit(solution)/shard_map/psum | solution.py:32
  35.8 34.0 %all-reduce.7.cloned.1.call-done = (bf16[64,1536]{1,0:T(8,128)(2,1)}, bf16[64,1536]{1,0:T(8,128)(2,1)}) async-done(((bf16[64,1536]{1,0:T(8,128)(2,1)}, bf16[64,1536]{1,0:T(8,128)(2,1)}), (bf16[64,1536]{1,0:T(8,128)(2,1)}, bf16[64,1536]{1,0:T(8,128)(2,1)})) %all-reduce.7.cloned.1.call-update) | async-done | bytes 393232 | tf_op jit(solution)/shard_map/psum | solution.py:31
  69.8 2.8 %fusion = bf16[1024,64]{0,1:T(8,128)(2,1)S(1)} fusion(bf16[1536,1024]{1,0:T(8,128)(2,1)} %param.27, bf16[64,1536]{1,0:T(8,128)(2,1)} %get-tuple-element.8, bf16[64,1536]{1,0:T(8,128)(2,1)} %get-tuple-element.9, f32[64]{0:T(128)S(1)} %add_rsqrt_fusion.2), kind=kOutput, calls=%fused_computation.8 | convolution fusion | flops 202375168 | bytes 3670272 | tf_op jit(solution)/shard_map/dot_general | solution.py:36
  72.6 0.8 copy.83
  73.5 30.9 %reduce-scatter.7.cloned.1.call-done = bf16[128,64]{1,0:T(8,128)(2,1)} async-done(((bf16[1024,64]{1,0:T(8,128)(2,1)}), bf16[128,64]{1,0:T(8,128)(2,1)}) %reduce-scatter.7.cloned.1.call-update) | async-done | bytes 16400
  104.4 0.8 copy.84
  107.1 3.7 %all-to-all-start = ((bf16[4,2,1024]{2,1,0:T(2,128)(2,1)}), bf16[4,2,1024]{2,1,0:T(2,128)(2,1)S(1)}, u32[]{:S(2)}, u32[]{:S(2)}) async-start(bf16[4,2,1024]{2,1,0:T(2,128)(2,1)} %reshape.81), calls=%async_computation | async-start | bytes 32768 | tf_op jit(solution)/shard_map/all_to_all | solution.py:75
  110.8 4.7 %all-to-all-done = bf16[4,2,1024]{2,1,0:T(2,128)(2,1)S(1)} async-done(((bf16[4,2,1024]{2,1,0:T(2,128)(2,1)}), bf16[4,2,1024]{2,1,0:T(2,128)(2,1)S(1)}, u32[]{:S(2)}, u32[]{:S(2)}) %all-to-all-start) | async-done | bytes 16416 | tf_op jit(solution)/shard_map/all_to_all | solution.py:75
  115.5 12.8 %all-gather = bf16[16,4,1,1024]{3,0,1,2:T(8,128)(2,1)S(1)} all-gather(bf16[16,4,1,128]{3,0,1,2:T(8,128)(2,1)S(1)} %bitcast.80), channel_id=2, replica_groups=mesh['kv'=4,'tp'=8] {'tp'}, dimensions={3}, use_global_device_ids=true | all-gather | bytes 147456 | tf_op jit(solution)/shard_map/all_gather | solution.py:78
  128.8 1.9 fusion.2
  130.9 2.8 %convolution_multiply_fusion = f32[16,512]{1,0:T(8,128)S(1)} fusion(bf16[16,4096]{1,0:T(8,128)(2,1)S(1)} %multiply_convert_fusion.3, bf16[4096,512]{1,0:T(8,128)(2,1)} %param.31, f32[16]{0:T(128)S(1)} %add_rsqrt_fusion.1), kind=kOutput, calls=%fused_computation.10 | convolution fusion | flops 67117056 | bytes 4358208 | tf_op jit(solution)/shard_map/dot_general | solution.py:88
  133.8 1.9 convolution_multiply_fusion.1
  136.0 1.1 fusion.28
  137.1 1.1 fusion.27
  139.2 5.8 %fusion.29 = f32[16,2,1,256]{3,2,1,0:T(1,128)S(1)} fusion(f32[16,2,128,1]{2,3,1,0:T(1,128)S(1)} %bitcast.78, f32[16,2,256,128]{3,2,1,0:T(8,128)} %param.21), kind=kOutput, calls=%fused_computation.62 | convolution fusion | flops 12582912 | bytes 4243456 | tf_op jit(solution)/shard_map/bhvd,bhd->bhv/dot_general | solution.py:102
  145.2 1.3 convolution_convert_fusion
  146.5 19.1 %all-gather.4.cloned.1.call-done = bf16[128,4096]{1,0:T(8,128)(2,1)} async-done(((bf16[16,4096]{1,0:T(8,128)(2,1)}), bf16[128,4096]{1,0:T(8,128)(2,1)}) %all-gather.4.cloned.1.call-update) | async-done | bytes 1048592 | tf_op jit(solution)/shard_map/all_gather | solution.py:10
  165.6 1.4 reduce_sum.61
  167.7 3.6 %all-to-all-start.1 = ((bf16[16,4,1024]{2,0,1:T(8,128)(2,1)}), bf16[16,4,1024]{2,0,1:T(8,128)(2,1)S(1)}, u32[]{:S(2)}, u32[]{:S(2)}) async-start(bf16[16,4,1024]{2,0,1:T(8,128)(2,1)} %fusion.5), calls=%async_computation.1 | async-start | bytes 262144 | tf_op jit(solution)/shard_map/all_to_all | solution.py:119
  172.0 4.3 %all-to-all-done.1 = bf16[16,4,1024]{2,0,1:T(8,128)(2,1)S(1)} async-done(((bf16[16,4,1024]{2,0,1:T(8,128)(2,1)}), bf16[16,4,1024]{2,0,1:T(8,128)(2,1)S(1)}, u32[]{:S(2)}, u32[]{:S(2)}) %all-to-all-start.1) | async-done | bytes 131104 | tf_op jit(solution)/shard_map/all_to_all | solution.py:119
  176.4 3.4 %convolution_convert_fusion.1 = bf16[64,1536]{1,0:T(8,128)(2,1)} fusion(bf16[1024,1536]{1,0:T(8,128)(2,1)} %param.38, bf16[64,1024]{1,0:T(8,128)(2,1)S(1)} %bitcast.71, f32[1024]{0:T(1024)S(1)} %dynamic_slice.19), kind=kOutput, calls=%fused_computation.2 | convolution fusion | flops 201621504 | bytes 3477504 | tf_op jit(solution)/shard_map/dot_general | solution.py:27
  179.7 1.3 convolution_convert_fusion.2
  181.3 8.5 %psum.45 = bf16[64]{0:T(256)(128)(2,1)S(1)} all-reduce(bf16[64]{0:T(256)(128)(2,1)S(1)} %convert_element_type.152), channel_id=1, replica_groups=mesh['kv'=4,'tp'=8] {'kv'}, use_global_device_ids=true, to_apply=%region_10.11 | all-reduce | flops 64 | bytes 256 | tf_op jit(solution)/shard_map/psum | solution.py:32
  189.8 33.8 %all-reduce.5.cloned.1.call-done = (bf16[64,1536]{1,0:T(8,128)(2,1)}, bf16[64,1536]{1,0:T(8,128)(2,1)}) async-done(((bf16[64,1536]{1,0:T(8,128)(2,1)}, bf16[64,1536]{1,0:T(8,128)(2,1)}), (bf16[64,1536]{1,0:T(8,128)(2,1)}, bf16[64,1536]{1,0:T(8,128)(2,1)})) %all-reduce.5.cloned.1.call-update) | async-done | bytes 393232 | tf_op jit(solution)/shard_map/psum | solution.py:31
  223.6 2.8 %fusion.1 = bf16[1024,64]{0,1:T(8,128)(2,1)S(1)} fusion(bf16[1536,1024]{1,0:T(8,128)(2,1)} %param.39, bf16[64,1536]{1,0:T(8,128)(2,1)} %get-tuple-element.6, bf16[64,1536]{1,0:T(8,128)(2,1)} %get-tuple-element.7, f32[64]{0:T(128)S(1)} %add_rsqrt_fusion), kind=kOutput, calls=%fused_computation.9 | convolution fusion | flops 202375168 | bytes 3670272 | tf_op jit(solution)/shard_map/dot_general | solution.py:36
  227.2 4.2 %multiply_add_fusion = f32[16,2,256,128]{3,2,1,0:T(8,128)} fusion(f32[16,2,256,128]{3,2,1,0:T(8,128)} %param.21, f32[16,2,128]{2,1,0:T(2,128)S(1)} %reshape.65, f32[16,2,256]{2,1,0:T(2,128)S(1)} %get-tuple-element.15, f32[16,2]{1,0:T(8,128)S(1)} %copy.69), kind=kLoop, calls=%fused_computation.1 | loop fusion | flops 3145728 | bytes 8437888 | tf_op jit(solution)/shard_map/add | solution.py:112
  232.2 26.0 %reduce-scatter.9.cloned.1.call-done = bf16[128,64]{1,0:T(8,128)(2,1)} async-done(((bf16[1024,64]{1,0:T(8,128)(2,1)}), bf16[128,64]{1,0:T(8,128)(2,1)}) %reduce-scatter.9.cloned.1.call-update) | async-done | bytes 16400
  258.2 0.8 copy.86
  (64 shorter events, 8.0 us)
Async XLA Ops:
  7.2 15.8 %copy-start = (bf16[1024,1536]{1,0:T(8,128)(2,1)S(1)}, bf16[1024,1536]{1,0:T(8,128)(2,1)}, u32[]{:S(2)}) copy-start(bf16[1024,1536]{1,0:T(8,128)(2,1)} %param.26) | copy-start | bytes 9437188
  7.2 62.6 %all-reduce.7.cloned.1.call-start = ((), (), s32[]{:S(2)}) async-start(), calls=%async_computation.8 | async-start | bytes 786432 | tf_op jit(solution)/shard_map/psum | solution.py:31
  22.1 2.2 copy-start.2
  25.6 79.7 %copy-start.4 = (bf16[64,128]{1,0:T(8,128)(2,1)S(1)}, bf16[64,128]{1,0:T(8,128)(2,1)}, u32[]{:S(2)}) copy-start(bf16[64,128]{1,0:T(8,128)(2,1)} %param.20) | copy-start | bytes 49156
  25.6 78.8 %reduce-scatter.7.cloned.1.call-start = ((), (), s32[]{:S(2)}) async-start(), calls=%async_computation.5 | async-start | bytes 294912
  69.8 59.0 %copy-start.6 = (f32[4096]{0:T(1024)S(1)}, f32[4096]{0:T(1024)}, u32[]{:S(2)}) copy-start(f32[4096]{0:T(1024)} %param.28) | copy-start | bytes 49156
  107.1 8.4 %all-to-all-start = ((bf16[4,2,1024]{2,1,0:T(2,128)(2,1)}), bf16[4,2,1024]{2,1,0:T(2,128)(2,1)S(1)}, u32[]{:S(2)}, u32[]{:S(2)}) async-start(bf16[4,2,1024]{2,1,0:T(2,128)(2,1)} %reshape.81), calls=%async_computation | async-start | bytes 32768 | tf_op jit(solution)/shard_map/all_to_all | solution.py:75
  110.8 54.8 %all-gather.4.cloned.1.call-start = ((), (), s32[]{:S(2)}) async-start(), calls=%async_computation.4 | async-start | bytes 1179648 | tf_op jit(solution)/shard_map/all_gather | solution.py:10
  130.8 4.9 %copy-start.5 = (f32[16,2,128]{2,1,0:T(2,128)S(1)}, f32[16,2,128]{2,1,0:T(2,128)}, u32[]{:S(2)}) copy-start(f32[16,2,128]{2,1,0:T(2,128)} %param.22) | copy-start | bytes 49156
  130.9 7.3 %copy-start.7 = (f32[16,2]{0,1:T(2,128)S(1)}, f32[16,2]{0,1:T(2,128)}, u32[]{:S(2)}) copy-start(f32[16,2]{0,1:T(2,128)} %param.23) | copy-start | bytes 388
  130.9 7.3 %copy-start.8 = (f32[2]{0:T(128)S(1)}, f32[2]{0:T(128)}, u32[]{:S(2)}) copy-start(f32[2]{0:T(128)} %param.34) | copy-start | bytes 28
  139.2 6.0 %copy-start.1 = (bf16[512,4096]{1,0:T(8,128)(2,1)S(1)}, bf16[512,4096]{1,0:T(8,128)(2,1)}, u32[]{:S(2)}) copy-start(bf16[512,4096]{1,0:T(8,128)(2,1)} %param.35) | copy-start | bytes 12582916
  167.7 8.7 %all-to-all-start.1 = ((bf16[16,4,1024]{2,0,1:T(8,128)(2,1)}), bf16[16,4,1024]{2,0,1:T(8,128)(2,1)S(1)}, u32[]{:S(2)}, u32[]{:S(2)}) async-start(bf16[16,4,1024]{2,0,1:T(8,128)(2,1)} %fusion.5), calls=%async_computation.1 | async-start | bytes 262144 | tf_op jit(solution)/shard_map/all_to_all | solution.py:119
  171.3 52.2 %all-reduce.5.cloned.1.call-start = ((), (), s32[]{:S(2)}) async-start(), calls=%async_computation.7 | async-start | bytes 786432 | tf_op jit(solution)/shard_map/psum | solution.py:31
  176.4 3.4 %copy-start.3 = (bf16[1024,1536]{1,0:T(8,128)(2,1)S(1)}, bf16[1024,1536]{1,0:T(8,128)(2,1)}, u32[]{:S(2)}) copy-start(bf16[1024,1536]{1,0:T(8,128)(2,1)} %param.37) | copy-start | bytes 9437188
  181.1 77.1 %reduce-scatter.9.cloned.1.call-start = ((), (), s32[]{:S(2)}) async-start(), calls=%async_computation.6 | async-start | bytes 294912
Sparse Core Ops, SparseCore 0:
  25.7 44.0 all-reduce.6
  73.6 30.7 reduce-scatter.6
  146.7 18.8 all-gather.3
  181.2 42.3 all-reduce.4
  227.4 30.7 reduce-scatter.8
